TPU v7x, 512 devices: a whole 4x8x8 slice. The times are simulated.
512 devices in a mesh: ep: 32 (over z, x), tp: 16 (over y, core).
Axes of the slice: x: 4, y: 8, z: 8, core: 2. Of those that a mesh axis runs over, the one named last changes fastest.
Arguments:
- tokens: bfloat16 [768, 4096], P('ep'), may hold values from -6 to 6
- norm_gain: float32 [4096], replicated, may hold values from 0.1 to 1.9
- routes: int32 [768, 6], P('ep'), may hold values from 0 to 63, all different within a row; in each aligned block of 24 rows (0 to 23, 24 to 47, ...) at most 6 rows name the same one
- route_scores: float32 [768, 6], P('ep'), may hold values from 0.05 to 1
- expert_gate: bfloat16 [64, 1024, 4096], P('ep', 'tp'), may hold values from -0.09375 to 0.09375
- expert_up: bfloat16 [64, 1024, 4096], P('ep', 'tp'), may hold values from -0.09375 to 0.09375
- expert_down: bfloat16 [64, 1024, 4096], P('ep', 'tp'), may hold values from -0.1875 to 0.1875
- shared_gate: bfloat16 [1024, 4096], P('tp'), may hold values from -0.09375 to 0.09375
- shared_up: bfloat16 [1024, 4096], P('tp'), may hold values from -0.09375 to 0.09375
- shared_down: bfloat16 [1024, 4096], P('tp'), may hold values from -0.1875 to 0.1875
Outputs:
- mixed: bfloat16 [768, 4096], P('ep', 'tp')
Inputs may be any that keep to these rules, and one draw needn't show every extreme that they name: `routes`: each row names 6 different experts. In the rows of one device (aligned blocks of 24 rows) no expert is named by more than 6 rows, and in some block one expert is named by exactly 6 rows.
All inputs are finite; a program needn't handle non-finite values.
Results may differ from a plain program's by a relative error of at most 0.02.
Values may be sent and summed in bfloat16 or wider, within the bound.
No kernel may reach another device: no remote copies, remote signals or barrier semaphores. Data moves between devices by JAX's collectives and lax.ppermute only.
A program may use at most 64 MiB of HBM per device.

v0:
```python
import jax
import jax.numpy as jnp
from jax import lax
from jax.sharding import PartitionSpec as P


def in_one_piece(arrays, axis, dim, along):
    widths = [a.shape[along] for a in arrays]
    both = jnp.concatenate(arrays, axis=along)
    filled = lax.psum_scatter(both, axis, scatter_dimension=dim, tiled=True)
    return tuple(jnp.split(filled, [sum(widths[:k]) for k in range(1, len(widths))], axis=along))


def capacity(tok_rows, chosen, experts):
    return min(tok_rows, max(4, 2 * ((tok_rows * chosen + experts - 1) // experts)))


def slot_index(route_block, experts, slot_count):
    flat = route_block.reshape(-1)
    onehot = (flat[:, None] == jnp.arange(experts, dtype=jnp.int32)[None, :]).astype(jnp.int32)
    before = jnp.cumsum(onehot, 0) - onehot
    order = jnp.sum(before * onehot, 1)
    return (flat * slot_count + order).reshape(route_block.shape)


def rounded(values):
    return lax.optimization_barrier(values.astype(jnp.bfloat16)).astype(jnp.float32)


def body(
    tokens,
    norm_gain,
    routes,
    route_scores,
    expert_gate,
    expert_up,
    expert_down,
    shared_gate,
    shared_up,
    shared_down,
):
    tok_rows, width = tokens.shape
    chosen = routes.shape[1]
    ep_size = lax.axis_size("ep")
    local = expert_gate.shape[0]
    experts = local * ep_size
    slot_count = capacity(tok_rows, chosen, experts)
    values = tokens.astype(jnp.float32)
    normed = (
        values * lax.rsqrt(jnp.mean(values * values, -1, keepdims=True) + 1e-06) * norm_gain
    ).astype(jnp.bfloat16)
    slots = slot_index(routes, experts, slot_count)
    tp_size = lax.axis_size("tp")
    columns = width // tp_size
    cells = jnp.arange(experts * slot_count, dtype=jnp.int32)
    table = jnp.sum((slots[None, :, :] == cells[:, None, None]).astype(jnp.float32), 2).astype(
        jnp.bfloat16
    )
    own_cols = lax.dynamic_slice_in_dim(normed, lax.axis_index("tp") * columns, columns, 1)
    buffer = jnp.dot(table, own_cols, preferred_element_type=jnp.float32).astype(jnp.bfloat16)
    buffer = buffer.reshape(ep_size, local, slot_count, columns)
    arrived = lax.all_to_all(buffer, "ep", split_axis=0, concat_axis=0, tiled=True)
    piece = lax.all_gather(arrived, "tp", axis=3, tiled=True)
    gate = jnp.einsum("secd,efd->secf", piece, expert_gate, preferred_element_type=jnp.float32)
    upper = jnp.einsum("secd,efd->secf", piece, expert_up, preferred_element_type=jnp.float32)
    gate, upper = (gate, upper)
    hidden = (jax.nn.silu(gate) * upper).astype(jnp.bfloat16)
    partial_value = rounded(
        jnp.einsum("secf,efd->secd", hidden, expert_down, preferred_element_type=jnp.float32)
    )
    shared_g = jnp.einsum("td,fd->tf", normed, shared_gate, preferred_element_type=jnp.float32)
    shared_u = jnp.einsum("td,fd->tf", normed, shared_up, preferred_element_type=jnp.float32)
    shared_hidden = (jax.nn.silu(shared_g) * shared_u).astype(jnp.bfloat16)
    shared_part = rounded(jnp.dot(shared_hidden, shared_down, preferred_element_type=jnp.float32))
    summed, shared_out = tuple(
        (
            part.astype(jnp.float32)
            for part in in_one_piece(
                (
                    partial_value.reshape(-1, width).astype(jnp.bfloat16),
                    shared_part.astype(jnp.bfloat16),
                ),
                "tp",
                1,
                0,
            )
        )
    )
    expert_out = summed.astype(jnp.bfloat16).reshape(ep_size, local * slot_count, -1)
    returned = lax.all_to_all(expert_out, "ep", split_axis=0, concat_axis=0, tiled=True).reshape(
        experts * slot_count, -1
    )
    weights = route_scores / jnp.sum(route_scores, -1, keepdims=True) * 2.5
    every_slot = jnp.arange(experts * slot_count, dtype=jnp.int32)
    combine = jnp.sum(
        weights[:, :, None] * (slots[:, :, None] == every_slot[None, None, :]).astype(jnp.float32),
        1,
    )
    routed = jnp.dot(combine, returned.astype(jnp.float32))
    return (shared_out + routed).astype(jnp.bfloat16)


def solution(mesh):
    in_specs = (
        P("ep", None),
        P(),
        P("ep", None),
        P("ep", None),
        P("ep", "tp", None),
        P("ep", "tp", None),
        P("ep", "tp", None),
        P("tp", None),
        P("tp", None),
        P("tp", None),
    )
    out_specs = P("ep", "tp")
    return jax.shard_map(body, mesh=mesh, in_specs=in_specs, out_specs=out_specs, check_vma=False)
```

profile of v0, /device:TPU:25, one launch (start us, length us, event | category | flops | bytes accessed | tf_op | source)
XLA Modules:
  0.0 199.0 jit_solution(11321514032493120497)
XLA Ops:
  6.6 0.9 copy.46
  7.5 0.1 eq.48
  7.6 0.6 reduce-window.6
  8.2 0.2 slice_reduce_fusion
  8.4 0.1 bitcast_bitcast_fusion
  8.6 0.1 reduce_sum.48
  8.7 0.1 copy.49
  8.8 0.7 multiply_add_fusion
  9.5 0.1 convert_reduce_fusion
  9.6 1.1 fusion.9
  10.6 1.1 fusion.11
  11.7 0.2 convolution_convert_fusion.2
  12.0 0.1 reshape.49
  12.0 0.2 copy.50
  12.2 22.7 %all_to_all.10 = bf16[32,2,6,256]{3,1,2,0:T(2,128)(2,1)S(1)} all-to-all(bf16[32,2,6,256]{3,1,2,0:T(2,128)(2,1)S(1)} %copy.50), channel_id=1, replica_groups=mesh['ep'=32,'tp'=16] {'ep'}, dimensions={0} | all-to-all | bytes 393216 | tf_op jit(solution)/shard_map/all_to_all | solution.py:62
  34.9 0.7 copy.51
  35.6 0.0 reduce-scatter.2.cloned.1.call-start
  35.6 0.2 fusion.31
  35.9 1.8 convolution_convert_fusion.1
  37.7 41.6 %all-gather.2.cloned.1.call-done = bf16[32,2,6,4096]{3,0,2,1:T(8,128)(2,1)} async-done(((bf16[32,2,6,256]{3,0,2,1:T(8,128)(2,1)}), bf16[32,2,6,4096]{3,0,2,1:T(8,128)(2,1)}) %all-gather.2.cloned.1.call-update) | async-done | bytes 3145744 | tf_op jit(solution)/shard_map/all_gather | solution.py:63
  79.3 2.8 %convolution_bitcast_fusion.1 = f32[32,2,6,64]{3,0,2,1:T(8,128)S(1)} fusion(bf16[32,2,6,4096]{3,0,2,1:T(8,128)(2,1)} %all-gather.2.cloned.1.call-done, bf16[2,64,4096]{2,1,0:T(8,128)(2,1)S(1)} %copy-done.1), kind=kOutput, calls=%fused_computation.7 | convolution fusion | flops 201326592 | bytes 4292608 | tf_op jit(solution)/shard_map/secd,efd->secf/dot_general | solution.py:64
  82.2 5.7 %fusion = bf16[32,2,6,4096]{3,0,2,1:T(8,128)(2,1)} fusion(bf16[32,2,6,4096]{3,0,2,1:T(8,128)(2,1)} %all-gather.2.cloned.1.call-done, bf16[2,64,4096]{2,1,0:T(8,128)(2,1)S(1)} %copy-done, bf16[2,64,4096]{2,1,0:T(8,128)(2,1)} %param.15, f32[32,2,6,64]{3,0,2,1:T(8,128)S(1)} %convolution_bitcast_fusion.1), kind=kOutput, calls=%fused_computation.1 | convolution fusion | flops 404373504 | bytes 8486912 | tf_op jit(solution)/shard_map/secf,efd->secd/dot_general | solution.py:69
  87.9 5.6 %copy.52 = bf16[32,2,6,4096]{3,2,1,0:T(8,128)(2,1)} copy(bf16[32,2,6,4096]{3,0,2,1:T(8,128)(2,1)} %fusion) | data formatting | bytes 6291456 | tf_op jit(solution)/shard_map/optimization_barrier | solution.py:27
  93.5 5.7 %convert_element_type.60 = bf16[384,4096]{1,0:T(8,128)(2,1)} reshape(bf16[32,2,6,4096]{3,2,1,0:T(8,128)(2,1)} %copy.52) | data formatting | bytes 6291456 | tf_op jit(solution)/shard_map/convert_element_type | solution.py:80
  99.2 3.9 %pad_maximum_fusion = bf16[408,4096]{1,0:T(8,128)(2,1)} fusion(bf16[24,4096]{1,0:T(8,128)(2,1)S(1)} %convolution_convert_fusion.1, bf16[384,4096]{1,0:T(8,128)(2,1)} %convert_element_type.60), kind=kLoop, calls=%fused_computation.3 | loop fusion | flops 6684672 | bytes 6684672 | tf_op jit(solution)/shard_map/concatenate | solution.py:9
  103.2 64.6 %reduce-scatter.2.cloned.1.call-done = bf16[408,256]{1,0:T(8,128)(2,1)} async-done(((bf16[408,4096]{1,0:T(8,128)(2,1)}), bf16[408,256]{1,0:T(8,128)(2,1)}) %reduce-scatter.2.cloned.1.call-update) | async-done | bytes 208912 | tf_op jit(solution)/shard_map/reduce_scatter | solution.py:10
  167.8 0.9 split.9
  168.7 0.7 reshape.50
  169.5 9.9 %all-to-all-start.1 = ((bf16[32,12,256]{2,1,0:T(8,128)(2,1)}), bf16[32,12,256]{2,1,0:T(8,128)(2,1)S(1)}, u32[]{:S(2)}, u32[]{:S(2)}) async-start(bf16[32,12,256]{2,1,0:T(8,128)(2,1)} %reshape.50), calls=%async_computation.2 | async-start | bytes 524288 | tf_op jit(solution)/shard_map/all_to_all | solution.py:90
  179.4 0.1 select_reduce_fusion
  179.5 11.1 %all-to-all-done.1 = bf16[32,12,256]{2,1,0:T(8,128)(2,1)S(1)} async-done(((bf16[32,12,256]{2,1,0:T(8,128)(2,1)}), bf16[32,12,256]{2,1,0:T(8,128)(2,1)S(1)}, u32[]{:S(2)}, u32[]{:S(2)}) %all-to-all-start.1) | async-done | bytes 196640 | tf_op jit(solution)/shard_map/all_to_all | solution.py:90
  190.7 1.5 fusion.3
  (20 shorter events, 0.2 us)
Async XLA Ops:
  6.5 75.6 %copy-start = (bf16[2,64,4096]{2,1,0:T(8,128)(2,1)S(1)}, bf16[2,64,4096]{2,1,0:T(8,128)(2,1)}, u32[]{:S(2)}) copy-start(bf16[2,64,4096]{2,1,0:T(8,128)(2,1)} %param.16) | copy-start | bytes 3145732
  6.5 29.1 %copy-start.2 = (bf16[64,4096]{1,0:T(8,128)(2,1)S(1)}, bf16[64,4096]{1,0:T(8,128)(2,1)}, u32[]{:S(2)}) copy-start(bf16[64,4096]{1,0:T(8,128)(2,1)} %param.17) | copy-start | bytes 1572868
  6.5 72.8 %copy-start.1 = (bf16[2,64,4096]{2,1,0:T(8,128)(2,1)S(1)}, bf16[2,64,4096]{2,1,0:T(8,128)(2,1)}, u32[]{:S(2)}) copy-start(bf16[2,64,4096]{2,1,0:T(8,128)(2,1)} %param.14) | copy-start | bytes 3145732
  6.5 72.8 %all-gather.2.cloned.1.call-start = ((), (), s32[]{:S(2)}) async-start(), calls=%async_computation.3 | async-start | bytes 3342336 | tf_op jit(solution)/shard_map/all_gather | solution.py:63
  35.6 132.2 %reduce-scatter.2.cloned.1.call-start = ((), (), s32[]{:S(2)}) async-start(), calls=%async_computation.4 | async-start | bytes 3551232 | tf_op jit(solution)/shard_map/reduce_scatter | solution.py:10
  103.1 76.3 %copy-start.3 = (f32[24,6]{0,1:T(8,128)S(1)}, f32[24,6]{0,1:T(8,128)}, u32[]{:S(2)}) copy-start(f32[24,6]{0,1:T(8,128)} %param.13) | copy-start | bytes 1732
  169.5 21.1 %all-to-all-start.1 = ((bf16[32,12,256]{2,1,0:T(8,128)(2,1)}), bf16[32,12,256]{2,1,0:T(8,128)(2,1)S(1)}, u32[]{:S(2)}, u32[]{:S(2)}) async-start(bf16[32,12,256]{2,1,0:T(8,128)(2,1)} %reshape.50), calls=%async_computation.2 | async-start | bytes 524288 | tf_op jit(solution)/shard_map/all_to_all | solution.py:90
Sparse Core Ops, SparseCore 0:
  35.7 43.5 all-gather.1
  103.3 64.4 reduce-scatter.1
where the time goes:
time: 200 us; the launch traced here: 199 us
  waiting for transfers between devices  117 us (58%)
  blocking collectives  22.7 us (11%)
  local copies, waits for them, and re-layouts  15.3 us (8%)
  between operations  13.6 us (7%)
  matrix products  12.3 us (6%)
  starting transfers between devices  9.94 us (5%)
  other arithmetic  7.8 us (4%)
    reduce_scatter x1, waiting for transfers between devices, in_one_piece(): filled = lax.psum_scatter(both, axis, scatter_dimension=dim, tiled=True)  64.6 us
    all_gather x1, waiting for transfers between devices, body(): piece = lax.all_gather(arrived, 'tp', axis=3, tiled=True)  41.6 us
    all_to_all x1, blocking collectives, body(): lax.all_to_all(buffer, 'ep', split_axis=0, concat_axis=0, tiled=True)  22.7 us
    all_to_all x1, waiting for transfers between devices, body(): lax.all_to_all(expert_out, 'ep', split_axis=0, concat_axis=0, tiled=True)  11.1 us
    all_to_all x1, starting transfers between devices, body(): lax.all_to_all(expert_out, 'ep', split_axis=0, concat_axis=0, tiled=True)  9.9 us
    convert_element_type x1, local copies, waits for them, and re-layouts, body(): partial_value.reshape(-1, width).astype(jnp.bfloat16)  5.73 us
    dot_general x1, matrix products, body(): jnp.einsum('secf,efd->secd', hidden, expert_down, preferred_element_type=...  5.72 us
    optimization_barrier x1, local copies, waits for them, and re-layouts, rounded(): lax.optimization_barrier(values.astype(jnp.bfloat16)).astype(jnp.float32)  5.57 us
  transfers between devices with their start and end apart: 3, of which 3 were waited for; matrix products, arithmetic and copies ran while one was open for 1% of the time, Pallas kernels for 0%

commit v1 on v0

--- a/solution.py
+++ b/solution.py
@@ -60,7 +60,14 @@
     buffer = jnp.dot(table, own_cols, preferred_element_type=jnp.float32).astype(jnp.bfloat16)
     buffer = buffer.reshape(ep_size, local, slot_count, columns)
     arrived = lax.all_to_all(buffer, "ep", split_axis=0, concat_axis=0, tiled=True)
-    piece = lax.all_gather(arrived, "tp", axis=3, tiled=True)
+
+    def wait_masks(k_dim, block_here):
+        long_array = jnp.concatenate(
+            lax.all_to_all(jnp.stack(lax.axis_size("tp") * [block_here]), "tp", 0, 0), axis=k_dim
+        )
+        return long_array
+
+    piece = wait_masks(3, arrived)
     gate = jnp.einsum("secd,efd->secf", piece, expert_gate, preferred_element_type=jnp.float32)
     upper = jnp.einsum("secd,efd->secf", piece, expert_up, preferred_element_type=jnp.float32)
     gate, upper = (gate, upper)

time: 200 us -> 233 us (1.17)
  waiting for transfers between devices: 117 us -> 139 us
  starting transfers between devices: 9.94 us -> 19.6 us
  local copies, waits for them, and re-layouts: 15.3 us -> 20.7 us
  matrix products: 12.3 us -> 8.92 us
    all_to_all x0 -> x1, waiting for transfers between devices: none -> 70.3 us  [wait_masks(): lax.all_to_all(jnp.stack(lax.axis_size('tp') * [block_here]), 'tp', 0, 0)]
    all_gather x1 -> x0, waiting for transfers between devices: 41.6 us -> none  [body(): piece = lax.all_gather(arrived, 'tp', axis=3, tiled=True)]
    all_to_all x0 -> x1, starting transfers between devices: none -> 9.7 us  [wait_masks(): lax.all_to_all(jnp.stack(lax.axis_size('tp') * [block_here]), 'tp', 0, 0)]
    reduce_scatter x1, waiting for transfers between devices: 64.6 us -> 57.5 us  [in_one_piece(): filled = lax.psum_scatter(both, axis, scatter_dimension=dim, tiled=True)]
    reshape x0 -> x1, local copies, waits for them, and re-layouts: none -> 2.37 us  [wait_masks(): jnp.concatenate(lax.all_to_all(jnp.stack(lax.axis_size('tp') * [block_her...]
  transfers between devices with their start and end apart: 3 -> 3, of which waited for: 3 -> 3; matrix products, arithmetic and copies ran while one was open for 1% -> 0% of each run, Pallas kernels for 0% -> 0%
where the time goes in v1:
time: 233 us; the launch traced here: 232 us
  waiting for transfers between devices  139 us (60%)
  blocking collectives  22.7 us (10%)
  local copies, waits for them, and re-layouts  20.7 us (9%)
  starting transfers between devices  19.6 us (8%)
  between operations  13.6 us (6%)
  matrix products  8.92 us (4%)
  other arithmetic  7.8 us (3%)
    all_to_all x1, waiting for transfers between devices, wait_masks(): lax.all_to_all(jnp.stack(lax.axis_size('tp') * [block_here]), 'tp', 0, 0)  70.3 us
    reduce_scatter x1, waiting for transfers between devices, in_one_piece(): filled = lax.psum_scatter(both, axis, scatter_dimension=dim, tiled=True)  57.5 us
    all_to_all x1, blocking collectives, body(): lax.all_to_all(buffer, 'ep', split_axis=0, concat_axis=0, tiled=True)  22.7 us
    all_to_all x1, waiting for transfers between devices, body(): lax.all_to_all(expert_out, 'ep', split_axis=0, concat_axis=0, tiled=True)  11.1 us
    all_to_all x1, starting transfers between devices, body(): lax.all_to_all(expert_out, 'ep', split_axis=0, concat_axis=0, tiled=True)  9.89 us
    all_to_all x1, starting transfers between devices, wait_masks(): lax.all_to_all(jnp.stack(lax.axis_size('tp') * [block_here]), 'tp', 0, 0)  9.7 us
    convert_element_type x1, local copies, waits for them, and re-layouts, body(): partial_value.reshape(-1, width).astype(jnp.bfloat16)  5.73 us
    optimization_barrier x1, local copies, waits for them, and re-layouts, rounded(): lax.optimization_barrier(values.astype(jnp.bfloat16)).astype(jnp.float32)  5.57 us
  transfers between devices with their start and end apart: 3, of which 3 were waited for; matrix products, arithmetic and copies ran while one was open for 0% of the time, Pallas kernels for 0%

profile of v1, /device:TPU:25, one launch (start us, length us, event | category | flops | bytes accessed | tf_op | source)
XLA Modules:
  0.0 232.3 jit_solution(1607759236930833635)
XLA Ops:
  6.5 0.9 copy.41
  7.4 0.1 eq.48
  7.5 0.6 reduce-window.6
  8.1 0.2 slice_reduce_fusion
  8.4 0.1 bitcast_bitcast_fusion
  8.5 0.1 reduce_sum.48
  8.7 0.7 multiply_add_fusion
  9.4 0.1 convert_reduce_fusion
  9.5 1.1 fusion.9
  10.6 1.1 fusion.11
  11.6 0.2 convolution_convert_fusion.2
  12.0 0.2 copy.45
  12.1 22.7 %all_to_all.15 = bf16[32,2,6,256]{3,1,2,0:T(2,128)(2,1)S(1)} all-to-all(bf16[32,2,6,256]{3,1,2,0:T(2,128)(2,1)S(1)} %copy.45), channel_id=1, replica_groups=mesh['ep'=32,'tp'=16] {'ep'}, dimensions={0} | all-to-all | bytes 393216 | tf_op jit(solution)/shard_map/all_to_all | solution.py:62
  34.8 2.1 stack.2
  36.9 9.7 %all-to-all-start.1 = ((bf16[16,32,2,6,256]{4,1,3,2,0:T(8,128)(2,1)}), bf16[16,32,2,6,256]{4,1,3,2,0:T(8,128)(2,1)}, u32[]{:S(2)}, u32[]{:S(2)}) async-start(bf16[16,32,2,6,256]{4,1,3,2,0:T(8,128)(2,1)} %stack.2), calls=%async_computation.1 | async-start | bytes 6291456 | tf_op jit(solution)/shard_map/all_to_all | solution.py:66
  46.7 0.2 fusion.31
  46.9 0.6 convolution_convert_fusion.1
  47.5 70.3 %all-to-all-done.1 = bf16[16,32,2,6,256]{4,1,3,2,0:T(8,128)(2,1)} async-done(((bf16[16,32,2,6,256]{4,1,3,2,0:T(8,128)(2,1)}), bf16[16,32,2,6,256]{4,1,3,2,0:T(8,128)(2,1)}, u32[]{:S(2)}, u32[]{:S(2)}) %all-to-all-start.1) | async-done | bytes 3145760 | tf_op jit(solution)/shard_map/all_to_all | solution.py:66
  117.9 2.4 %copy.54 = bf16[16,2,6,4,8,256]{5,4,0,3,2,1:T(8,128)(2,1)S(1)} copy(bf16[16,2,6,4,8,256]{5,4,3,2,1,0:T(8,128)(2,1)} %bitcast.18) | data formatting | bytes 6291456 | tf_op jit(solution)/shard_map/reshape | solution.py:65
  120.3 1.7 copy-done.1
  121.9 1.0 convolution_bitcast_fusion.1
  122.9 5.4 %fusion = bf16[32,2,6,4096]{3,0,2,1:T(8,128)(2,1)} fusion(bf16[32,2,6,4096]{3,0,2,1:T(8,128)(2,1)} %bitcast.54, bf16[2,64,4096]{2,1,0:T(8,128)(2,1)S(1)} %copy-done, bf16[2,64,4096]{2,1,0:T(8,128)(2,1)S(1)} %copy-done.3, f32[32,2,6,64]{3,0,2,1:T(8,128)S(1)} %convolution_bitcast_fusion.1), kind=kOutput, calls=%fused_computation.1 | convolution fusion | flops 404373504 | bytes 8486912 | tf_op jit(solution)/shard_map/secf,efd->secd/dot_general | solution.py:76
  128.3 5.6 %copy.48 = bf16[32,2,6,4096]{3,2,1,0:T(8,128)(2,1)} copy(bf16[32,2,6,4096]{3,0,2,1:T(8,128)(2,1)} %fusion) | data formatting | bytes 6291456 | tf_op jit(solution)/shard_map/optimization_barrier | solution.py:27
  133.9 5.7 %convert_element_type.60 = bf16[384,4096]{1,0:T(8,128)(2,1)} reshape(bf16[32,2,6,4096]{3,2,1,0:T(8,128)(2,1)} %copy.48) | data formatting | bytes 6291456 | tf_op jit(solution)/shard_map/convert_element_type | solution.py:87
  139.6 3.9 %pad_maximum_fusion = bf16[408,4096]{1,0:T(8,128)(2,1)} fusion(bf16[24,4096]{1,0:T(8,128)(2,1)S(1)} %convolution_convert_fusion.1, bf16[384,4096]{1,0:T(8,128)(2,1)} %convert_element_type.60), kind=kLoop, calls=%fused_computation.3 | loop fusion | flops 6684672 | bytes 6684672 | tf_op jit(solution)/shard_map/concatenate | solution.py:9
  143.6 57.5 %reduce-scatter.2.cloned.1.call-done = bf16[408,256]{1,0:T(8,128)(2,1)} async-done(((bf16[408,4096]{1,0:T(8,128)(2,1)}), bf16[408,256]{1,0:T(8,128)(2,1)}) %reduce-scatter.2.cloned.1.call-update) | async-done | bytes 208912 | tf_op jit(solution)/shard_map/reduce_scatter | solution.py:10
  201.1 0.9 split.9
  202.1 0.7 reshape.60
  202.8 9.9 %all-to-all-start.2 = ((bf16[32,12,256]{2,1,0:T(8,128)(2,1)}), bf16[32,12,256]{2,1,0:T(8,128)(2,1)S(1)}, u32[]{:S(2)}, u32[]{:S(2)}) async-start(bf16[32,12,256]{2,1,0:T(8,128)(2,1)} %reshape.60), calls=%async_computation.3 | async-start | bytes 524288 | tf_op jit(solution)/shard_map/all_to_all | solution.py:97
  212.8 0.1 select_reduce_fusion
  212.9 11.1 %all-to-all-done.2 = bf16[32,12,256]{2,1,0:T(8,128)(2,1)S(1)} async-done(((bf16[32,12,256]{2,1,0:T(8,128)(2,1)}), bf16[32,12,256]{2,1,0:T(8,128)(2,1)S(1)}, u32[]{:S(2)}, u32[]{:S(2)}) %all-to-all-start.2) | async-done | bytes 196640 | tf_op jit(solution)/shard_map/all_to_all | solution.py:97
  224.0 1.5 fusion.3
  (29 shorter events, 0.4 us)
Async XLA Ops:
  6.5 116.4 %copy-start = (bf16[2,64,4096]{2,1,0:T(8,128)(2,1)S(1)}, bf16[2,64,4096]{2,1,0:T(8,128)(2,1)}, u32[]{:S(2)}) copy-start(bf16[2,64,4096]{2,1,0:T(8,128)(2,1)} %param.16) | copy-start | bytes 3145732
  36.9 9.8 %copy-start.4 = (bf16[64,4096]{1,0:T(8,128)(2,1)S(1)}, bf16[64,4096]{1,0:T(8,128)(2,1)}, u32[]{:S(2)}) copy-start(bf16[64,4096]{1,0:T(8,128)(2,1)} %param.17) | copy-start | bytes 1572868
  36.9 10.0 %copy-start.5 = (bf16[64,4096]{1,0:T(8,128)(2,1)S(1)}, bf16[64,4096]{1,0:T(8,128)(2,1)}, u32[]{:S(2)}) copy-start(bf16[64,4096]{1,0:T(8,128)(2,1)} %param.19) | copy-start | bytes 1572868
  36.9 10.0 %copy-start.6 = (bf16[64,4096]{1,0:T(8,128)(2,1)S(1)}, bf16[64,4096]{1,0:T(8,128)(2,1)}, u32[]{:S(2)}) copy-start(bf16[64,4096]{1,0:T(8,128)(2,1)} %param.18) | copy-start | bytes 1572868
  36.9 81.0 %all-to-all-start.1 = ((bf16[16,32,2,6,256]{4,1,3,2,0:T(8,128)(2,1)}), bf16[16,32,2,6,256]{4,1,3,2,0:T(8,128)(2,1)}, u32[]{:S(2)}, u32[]{:S(2)}) async-start(bf16[16,32,2,6,256]{4,1,3,2,0:T(8,128)(2,1)} %stack.2), calls=%async_computation.1 | async-start | bytes 6291456 | tf_op jit(solution)/shard_map/all_to_all | solution.py:66
  46.6 154.5 %reduce-scatter.2.cloned.1.call-start = ((), (), s32[]{:S(2)}) async-start(), calls=%async_computation.4 | async-start | bytes 3551232 | tf_op jit(solution)/shard_map/reduce_scatter | solution.py:10
  117.9 4.1 %copy-start.2 = (bf16[2,64,4096]{2,1,0:T(8,128)(2,1)S(1)}, bf16[2,64,4096]{2,1,0:T(8,128)(2,1)}, u32[]{:S(2)}) copy-start(bf16[2,64,4096]{2,1,0:T(8,128)(2,1)} %param.14) | copy-start | bytes 3145732
  120.2 1.7 copy-start.1
  120.3 2.6 %copy-start.3 = (bf16[2,64,4096]{2,1,0:T(8,128)(2,1)S(1)}, bf16[2,64,4096]{2,1,0:T(8,128)(2,1)}, u32[]{:S(2)}) copy-start(bf16[2,64,4096]{2,1,0:T(8,128)(2,1)} %param.15) | copy-start | bytes 3145732
  143.6 69.1 %copy-start.7 = (f32[24,6]{0,1:T(8,128)S(1)}, f32[24,6]{0,1:T(8,128)}, u32[]{:S(2)}) copy-start(f32[24,6]{0,1:T(8,128)} %param.13) | copy-start | bytes 1732
  202.8 21.1 %all-to-all-start.2 = ((bf16[32,12,256]{2,1,0:T(8,128)(2,1)}), bf16[32,12,256]{2,1,0:T(8,128)(2,1)S(1)}, u32[]{:S(2)}, u32[]{:S(2)}) async-start(bf16[32,12,256]{2,1,0:T(8,128)(2,1)} %reshape.60), calls=%async_computation.3 | async-start | bytes 524288 | tf_op jit(solution)/shard_map/all_to_all | solution.py:97
Sparse Core Ops, SparseCore 0:
  143.7 57.3 reduce-scatter.1
